TPU v7x, 32 devices: a whole 2x2x4 slice. The times are simulated.
32 devices in a mesh: ep: 8 (over z, x), tp: 4 (over y, core).
Axes of the slice: x: 2, y: 2, z: 4, core: 2. Of those that a mesh axis runs over, the one named last changes fastest.
Arguments:
- tokens: bfloat16 [64, 2048], P(('ep', 'tp')), may hold values from -6 to 6
- cache_keys: bfloat16 [64, 1024, 256], P(('ep', 'tp')), may hold values from -360 to 360
- cache_values: bfloat16 [64, 1024, 256], P(('ep', 'tp')), may hold values from -6 to 6
- cache_gates: float32 [64, 2, 1024], P(('ep', 'tp')), may hold values from -256 to 0, as said below
- lengths: int32 [64], P(('ep', 'tp')), may hold values from 1 to 1024, 32768 in all
- routes: int32 [64, 4], P(('ep', 'tp')), may hold values from 0 to 7, all different within a row; in each aligned block of 2 rows (0 to 1, 2 to 3, ...) no two rows name the same one
- route_logits: float32 [64, 4], P(('ep', 'tp')), may hold values from -6 to 6
- attn_gain: float32 [2048], replicated, may hold values from 0.1 to 1.9
- w_query: bfloat16 [2048, 2048], P(None, 'tp'), may hold values from -0.125 to 0.125
- w_keyval: bfloat16 [2048, 512], P(None, 'tp'), may hold values from -0.125 to 0.125
- w_forget: bfloat16 [2048, 2], replicated, may hold values from -0.125 to 0.125
- forget_bias: float32 [2], replicated, may hold values from -1 to 3
- w_out: bfloat16 [2048, 2048], P(None, 'tp'), may hold values from -0.125 to 0.125
- mix_gain: float32 [2048], replicated, may hold values from 0.1 to 1.9
- ffn_gain: float32 [2048], replicated, may hold values from 0.1 to 1.9
- w_gate: bfloat16 [8, 2048, 2048], P('ep', None, 'tp'), may hold values from -0.125 to 0.125
- w_lin: bfloat16 [8, 2048, 2048], P('ep', None, 'tp'), may hold values from -0.125 to 0.125
- gate_bias: float32 [8, 2048], P('ep', 'tp'), may hold values from -12 to 12
- lin_bias: float32 [8, 2048], P('ep', 'tp'), may hold values from -12 to 12
- w_down: bfloat16 [8, 2048, 2048], P('ep', 'tp'), may hold values from -0.125 to 0.125
- post_gain: float32 [2048], replicated, may hold values from 0.1 to 1.9
Outputs:
- updated: bfloat16 [64, 2048], P(('ep', 'tp'))
- new_entries: bfloat16 [64, 512], P(('ep', 'tp'))
Inputs may be any that keep to these rules, and one draw needn't show every extreme that they name: `cache_gates`: along the positions of each sequence and head the values never increase. The lengths of all sequences add up to 32768, and some sequence has exactly 1024. `routes`: each row names 4 different experts; among the rows of one device no expert is named twice; every expert is named by some row.
All inputs are finite; a program needn't handle non-finite values. No bound on the sum of `lengths` on one device may be relied on, other than what follows from the above.
Results may differ from a plain program's by a relative error of at most 0.014.
The roundings to bfloat16 on the way count: a program that leaves them out, or rounds other values in their place, can miss the bound.
Values may be sent and summed in bfloat16 or wider, within the bound.
No kernel may reach another device: no remote copies, remote signals or barrier semaphores. Data moves between devices by JAX's collectives and lax.ppermute only.
A program may use at most 64 MiB of HBM per device.

v0:
```python
import functools
import math

import jax
import jax.numpy as jnp
from jax import lax
from jax.experimental import pallas as pl
from jax.experimental.pallas import tpu as pltpu
from jax.sharding import PartitionSpec as P


HEADS = 16
KVH = 2
HDIM = 128
LANES = 128

NORM_EPS = 1e-06
SWIGLU_ALPHA = 1.702
SWIGLU_LIMIT = 7.0
NEG_LARGE = -1e30

LOAD_FLOPS = 50_000_000


F32 = jnp.float32
BF16 = jnp.bfloat16
VMEM = pltpu.VMEM
SMEM = pltpu.SMEM


def call(body, outs, args, smem=(), hbm=(), hbm_out=(), raw_out=(), scratch=(), flops=0):
    spaces = [
        SMEM if i in smem else pl.ANY if i in hbm else VMEM for i in range(len(args))
    ]
    args = [
        pltpu.with_memory_space_constraint(a, VMEM)
        if space is VMEM
        else pltpu.with_memory_space_constraint(a, pltpu.HBM)
        if space is pl.ANY
        else a
        for a, space in zip(args, spaces)
    ]
    room = 4 << 20
    for entry in scratch:
        if isinstance(entry, tuple):
            room += 2 * math.prod(entry[0]) * jnp.dtype(entry[1]).itemsize
    return pl.pallas_call(
        body,
        out_shape=[
            jax.ShapeDtypeStruct(shape, dtype) if i in (*hbm_out, *raw_out) else VMEM(shape, dtype)
            for i, (shape, dtype) in enumerate(outs)
        ],
        in_specs=[pl.BlockSpec(memory_space=space) for space in spaces],
        out_specs=[
            pl.BlockSpec(memory_space=pl.ANY if i in raw_out else VMEM) for i in range(len(outs))
        ],
        scratch_shapes=[
            VMEM(*entry) if isinstance(entry, tuple) else entry for entry in scratch
        ],
        compiler_params=pltpu.CompilerParams(vmem_limit_bytes=room),
        cost_estimate=pl.CostEstimate(flops=flops, transcendentals=0, bytes_accessed=0),
    )(*args)


def start_copies(sources, targets, sems, pieces):
    copies = []
    for source, target, cuts in zip(sources, targets, pieces):
        size = source.shape[0] // cuts
        for c in range(cuts):
            part = pl.ds(c * size, size)
            copies.append(
                pltpu.make_async_copy(source.at[part], target.at[part], sems.at[len(copies)])
            )
    for copy in copies:
        copy.start()
    return copies


def load_body(*refs, pieces):
    count = len(pieces)
    for copy in start_copies(refs[:count], refs[-count - 1 : -1], refs[-1], pieces):
        copy.wait()


def load(arrays, pieces, flops, after=(), out=()):
    return call(
        functools.partial(load_body, pieces=pieces),
        [(a.shape, a.dtype) for a in arrays],
        [*arrays, *after],
        hbm=[i for i in range(len(arrays)) if i not in out],
        raw_out=out,
        scratch=[pltpu.SemaphoreType.DMA((sum(pieces),))],
        flops=flops,
    )


def inverse_rms(values):
    return lax.rsqrt(jnp.mean(values * values, axis=-1, keepdims=True) + NORM_EPS)


def inverse_rms_all(values):
    return lax.rsqrt(jnp.mean(values * values, axis=(0, 1), keepdims=True) + NORM_EPS)


def clamped_unit(gate, linear):
    gate = jnp.minimum(gate, SWIGLU_LIMIT)
    linear = jnp.clip(linear, -SWIGLU_LIMIT, SWIGLU_LIMIT)
    return gate * jax.nn.sigmoid(SWIGLU_ALPHA * gate) * (linear + 1.0)


def peers(size):
    assert size & (size - 1) == 0
    return [[(j, j ^ k) for j in range(size)] for k in range(1, size)]


def swap_all(pieces):
    out = [pieces[0]]
    for k, perm in enumerate(peers(lax.axis_size("tp")), 1):
        out.append(lax.ppermute(pieces[k], "tp", perm))
    return out


def prepare_body(
    keys, cache_values, lengths, tokens, gain, w_forget, bias, gates, routes, logits, after,
    flipped, values, bias_out, hit_out, combine_out, pick_out, tok_out, sems,
):
    del after
    copies = start_copies([cache_values], [values], sems, (2,))
    for s in range(keys.shape[0]):
        flipped[s] = keys[s].T
    seqs, width = tokens.shape
    span = gates.shape[2]
    raw = tokens[...].astype(F32)
    normed = (raw * inverse_rms(raw) * gain[...]).astype(BF16).astype(F32)
    w_rows = w_forget[...].astype(F32)
    lane = lax.broadcasted_iota(jnp.int32, (KVH, span), 1)
    head = lax.broadcasted_iota(jnp.int32, (KVH, 1), 0)
    shift = jnp.zeros((KVH, 1), F32)
    for g in range(KVH):
        shift = jnp.where(head == g, bias[:, g : g + 1], shift)
    for s in range(seqs):
        logit = jnp.sum(normed[s : s + 1] * w_rows, axis=-1, keepdims=True) + shift
        forget = jnp.minimum(logit, 0.0) - jnp.log1p(jnp.exp(-jnp.abs(logit)))
        own_gates = gates[s]
        live = lengths[:, s : s + 1]
        last = jnp.sum(jnp.where(lane == live - 1, own_gates, 0.0), axis=-1, keepdims=True)
        bias_out[s] = jnp.where(lane < live, (last + forget) - own_gates, NEG_LARGE)
        for c in range(width // LANES):
            row = s * (width // LANES) + c
            tok_out[row : row + 1, :] = raw[s : s + 1, c * LANES : (c + 1) * LANES]
    chosen = routes[...]
    scores = logits[...]
    expo = jnp.exp(scores - jnp.max(scores, axis=-1, keepdims=True))
    probs = expo / jnp.sum(expo, axis=-1, keepdims=True)
    expert = lax.broadcasted_iota(jnp.int32, hit_out.shape, 1)
    hit = jnp.zeros(hit_out.shape, F32)
    combine = jnp.zeros(hit_out.shape, F32)
    for k in range(chosen.shape[1]):
        match = (chosen[:, k : k + 1] == expert).astype(F32)
        hit = hit + match
        combine = combine + probs[:, k : k + 1] * match
    pick_out[...] = (chosen[:, :1] == expert).astype(F32)
    hit_out[...] = hit
    combine_out[...] = combine
    for copy in copies:
        copy.wait()


def project_in_body(*refs, groups):
    near, (gain, w_query, w_keyval) = refs[:groups], refs[groups : groups + 3]
    outs, rows = refs[groups + 3 : -1], refs[-1]
    seqs = near[0].shape[0]
    for k in range(groups):
        rows[k * seqs : (k + 1) * seqs, :] = near[k][...].astype(F32)
    raw = rows[...]
    normed = (raw * inverse_rms(raw) * gain[...]).astype(BF16)
    query = jnp.dot(normed, w_query[...], preferred_element_type=F32).astype(BF16)
    pair = jnp.dot(normed, w_keyval[...], preferred_element_type=F32).astype(BF16)
    cols = query.shape[1]
    for k in range(groups):
        outs[k][:, :cols] = query[k * seqs : (k + 1) * seqs]
        outs[k][:, cols:] = pair[k * seqs : (k + 1) * seqs]


def attend_body(*refs, groups, cols):
    near, (keys, values, bias, hit) = refs[:groups], refs[groups : groups + 4]
    mixed_out, fresh_out, pieces, q_rows, mixed_rows = refs[groups + 4 :]
    here = lax.axis_index("tp")
    seqs, _ = near[0].shape
    share = HEADS // KVH
    scale = HDIM ** (-0.5)
    for k in range(groups):
        pieces[here ^ k] = near[k][...].astype(F32)
    fresh = jnp.concatenate([pieces[c][:, cols:] for c in range(groups)], axis=1)
    fresh_out[...] = fresh.astype(BF16)
    q_rows[...] = jnp.zeros(q_rows.shape, F32)
    for s in range(seqs):
        for h in range(HEADS):
            c, at = h * HDIM // cols, h * HDIM % cols
            g = h // share
            q_rows[s * HEADS + h : s * HEADS + h + 1, g * HDIM : (g + 1) * HDIM] = pieces[
                c, s : s + 1, at : at + HDIM
            ]
    head = lax.broadcasted_iota(jnp.int32, (HEADS, 1), 0)
    for s in range(seqs):
        query = q_rows[s * HEADS : (s + 1) * HEADS, :]
        new_key = fresh[s : s + 1, : KVH * HDIM]
        new_value = fresh[s : s + 1, KVH * HDIM :]
        raw = jnp.dot(query.astype(BF16), keys[s], preferred_element_type=F32)
        row_bias = bias[s, KVH - 1 : KVH, :]
        for g in range(KVH - 1):
            row_bias = jnp.where((head >= g * share) & (head < (g + 1) * share), bias[s, g : g + 1, :], row_bias)
        scores = raw * scale + row_bias
        own = jnp.sum(query * new_key, axis=-1, keepdims=True) * scale
        top = jnp.maximum(jnp.max(scores, axis=-1, keepdims=True), own)
        expo = jnp.exp(scores - top)
        own_expo = jnp.exp(own - top)
        total = 1.0 / (jnp.sum(expo, axis=-1, keepdims=True) + own_expo)
        weight = (expo * total).astype(BF16)
        own_weight = (own_expo * total).astype(BF16).astype(F32)
        mixed = jnp.dot(weight, values[s], preferred_element_type=F32) + own_weight * new_value
        for h in range(HEADS):
            g = h // share
            mixed_rows[s : s + 1, h * HDIM : (h + 1) * HDIM] = mixed[
                h : h + 1, g * HDIM : (g + 1) * HDIM
            ]
    full = HEADS * HDIM
    mixed_out[:, :full] = mixed_rows[:seqs, :].astype(BF16)
    mixed_out[:, full:] = hit[...].astype(BF16)


def project_out_body(*refs, groups, experts, fold):
    near, tokens, w_out = refs[:groups], refs[groups : 2 * groups], refs[2 * groups]
    out, mixed_rows, parts, hits = refs[2 * groups + 1 :]
    here = lax.axis_index("tp")
    seqs = near[0].shape[0]
    width, cols = w_out.shape
    lanes = cols // fold

    def keep(which, k, rows):
        for s in range(seqs):
            for a in range(fold):
                parts[which * seqs + s, pl.ds(a * groups + (here ^ k), 1), :] = rows[
                    s : s + 1, a * lanes : (a + 1) * lanes
                ]

    for k in range(groups):
        mixed_rows[k * seqs : (k + 1) * seqs, :] = near[k][:, :width].astype(F32)
        hit = near[k][:, width:].astype(F32)
        for s in range(seqs):
            for a in range(fold):
                hits[s, pl.ds(a * groups + (here ^ k), 1), :] = hit[s : s + 1]
        keep(1, k, tokens[k][:, pl.ds(pl.multiple_of(here * cols, LANES), cols)].astype(F32))
    projected = jnp.dot(mixed_rows[...].astype(BF16), w_out[...], preferred_element_type=F32)
    for k in range(groups):
        keep(0, k, projected[k * seqs : (k + 1) * seqs])
    rows = [parts[n] for n in range(2 * seqs)]
    marks = [hits[s] for s in range(seqs)]
    for e in range(experts):
        on = [marks[s][:, e : e + 1] > 0.5 for s in range(seqs)]
        for which in range(2):
            block = jnp.zeros(rows[0].shape, F32)
            for s in range(seqs):
                block = jnp.where(on[s], rows[which * seqs + s], block)
            block = block.astype(BF16)
            for j in range(which, groups, 2):
                out[e * groups + j] = block


def expert_body(
    arrived, other, mix_gain, ffn_gain, w_gate, w_lin, gate_bias, lin_bias, w_down, out, expert_in, answer,
    *, groups, experts, fold
):
    here = lax.axis_index("tp")
    lanes = arrived.shape[1]
    tall = fold * groups
    width = w_gate.shape[0]
    chunks = width // LANES
    side = chunks // groups
    per = lanes // LANES
    blocks, height = out.shape[1:3]
    pitch = blocks * 8
    even = (here & 1) == 0

    def tile(slot, c):
        at = slot * tall
        if not isinstance(slot, int):
            at = pl.multiple_of(at, 8)
        spot = (pl.ds(at, tall), pl.ds(c * LANES, LANES))
        mine, theirs = arrived[spot].astype(F32), other[spot].astype(F32)
        return jnp.where(even, mine, theirs), jnp.where(even, theirs, mine)

    def spot(chunk):
        return chunk // height * 8 + chunk % height

    if blocks * height > chunks + side:
        answer[...] = jnp.zeros(answer.shape, F32)
    span = max(8 // groups, 1)
    for first in range(0, experts, span):
        near = range(first, first + span)
        projected, tokens = [], []
        for j in range(groups):
            tiles = [[tile(i * groups + j, c) for i in near] for c in range(per)]
            for a in range(fold):
                for c in range(per):
                    rows = [
                        [pair[n][a * groups : (a + 1) * groups] for pair in tiles[c]] for n in range(2)
                    ]
                    projected.append(jnp.concatenate(rows[0], axis=0))
                    tokens.append(jnp.concatenate(rows[1], axis=0))
        projected = jnp.concatenate(projected, axis=1)
        tokens = jnp.concatenate(tokens, axis=1)
        residual = tokens + projected * inverse_rms(projected) * mix_gain[...]
        normed = residual * inverse_rms(residual) * ffn_gain[...]
        at, count = first * groups, span * groups
        expert_in[at : at + count, :] = normed.astype(BF16)
        for c in range(per):
            tiles = [tile(i * groups + here, c)[0] for i in near]
            for a in range(fold):
                answer[pl.ds(at * pitch + spot(chunks + a * per + c), count, stride=pitch), :] = (
                    jnp.concatenate([t[a * groups : (a + 1) * groups] for t in tiles], axis=0)
                )
    rows = expert_in[...]
    gate = jnp.dot(rows, w_gate[...], preferred_element_type=F32) + gate_bias[...]
    linear = jnp.dot(rows, w_lin[...], preferred_element_type=F32) + lin_bias[...]
    act = clamped_unit(gate, linear).astype(BF16)
    part = jnp.dot(act, w_down[...], preferred_element_type=F32)
    for c in range(chunks):
        answer[pl.ds(spot(c), groups * experts, stride=pitch), :] = part[
            :, c * LANES : (c + 1) * LANES
        ]
    for slot in range(groups * experts):
        for b in range(blocks):
            at = slot * pitch + b * 8
            out[slot, b] = answer[at : at + height, :].astype(BF16)


def finish_body(
    returned, tokens, combine, pick, mix_gain, post_gain, out, rows, moe, near, *, groups, experts
):
    seqs, width = out.shape
    chunks = width // LANES
    side = chunks // groups
    height = returned.shape[2]
    tall = chunks // height
    zero = jnp.zeros((height, LANES), F32)
    sums = [[zero] * tall for _ in range(seqs)]
    own = [[zero] * groups for _ in range(seqs)]
    for e in range(experts):
        picked = [jnp.broadcast_to(pick[s : s + 1, e : e + 1], zero.shape) for s in range(seqs)]
        shares = [jnp.broadcast_to(combine[s : s + 1, e : e + 1], zero.shape) for s in range(seqs)]
        for b in range(tall):
            total = zero
            for j in range(groups):
                total = total + returned[e * groups + j, b].astype(F32)
            total = total.astype(BF16).astype(F32)
            for s in range(seqs):
                sums[s][b] = sums[s][b] + shares[s] * total
        for j in range(groups):
            part = returned[e * groups + j, tall].astype(F32)
            for s in range(seqs):
                own[s][j] = own[s][j] + picked[s] * part
    for s in range(seqs):
        for b in range(tall):
            moe[b * height : (b + 1) * height, :] = sums[s][b]
        for j in range(groups):
            near[j * side : (j + 1) * side, :] = own[s][j][:side]
        projected, mixture = near[...], moe[...]
        residual = (
            tokens[s * chunks : (s + 1) * chunks, :]
            + projected * inverse_rms_all(projected) * mix_gain[...]
        )
        updated = residual + mixture * inverse_rms_all(mixture) * post_gain[...]
        for c in range(chunks):
            rows[s : s + 1, c * LANES : (c + 1) * LANES] = updated[c : c + 1, :]
    out[...] = rows[:seqs, :].astype(BF16)


def layer(
    tokens,
    cache_keys,
    cache_values,
    cache_gates,
    lengths,
    routes,
    route_logits,
    attn_gain,
    w_query,
    w_keyval,
    w_forget,
    forget_bias,
    w_out,
    mix_gain,
    ffn_gain,
    w_gate,
    w_lin,
    gate_bias,
    lin_bias,
    w_down,
    post_gain,
):
    groups = lax.axis_size("tp")
    experts = lax.axis_size("ep")
    both_axes = ("ep", "tp")
    seqs, width = tokens.shape
    span = cache_keys.shape[1]
    cols = w_query.shape[1]
    pair = w_keyval.shape[1]
    chunks = width // LANES
    slots = experts * groups
    out_cols = w_out.shape[1]
    fold = 2 if groups < 8 and out_cols % (2 * LANES) == 0 else 1
    marked = -(-experts // LANES) * LANES
    row = lambda gain: gain.reshape(1, width)
    block = lambda gain: gain.reshape(chunks, LANES)

    near_tokens = swap_all([tokens] * groups)
    w_query, w_keyval, keys = load([w_query, w_keyval, cache_keys], (2, 1, 2), LOAD_FLOPS)
    sent = call(
        functools.partial(project_in_body, groups=groups),
        [((seqs, cols + pair), BF16)] * groups,
        [*near_tokens, row(attn_gain), w_query, w_keyval],
        scratch=[((groups * seqs, width), F32)],
    )
    near = swap_all(sent)
    keys, values, bias, hit, combine, pick, own_tokens = call(
        prepare_body,
        [
            ((seqs, KVH * HDIM, span), BF16),
            (cache_values.shape, BF16),
            ((seqs, KVH, span), F32),
            ((seqs, marked), F32),
            ((seqs, marked), F32),
            ((seqs, marked), F32),
            ((seqs * chunks, LANES), F32),
        ],
        [
            keys,
            cache_values,
            lengths.reshape(1, seqs),
            tokens,
            row(attn_gain),
            w_forget.T,
            forget_bias.reshape(1, KVH),
            cache_gates,
            routes,
            route_logits,
            sent[0],
        ],
        hbm=(1,),
        scratch=[pltpu.SemaphoreType.DMA((2,))],
        flops=LOAD_FLOPS,
    )
    mixed, fresh = call(
        functools.partial(attend_body, groups=groups, cols=cols),
        [((seqs, width + marked), BF16), ((seqs, 2 * KVH * HDIM), BF16)],
        [*near, keys, values, bias, hit],
        scratch=[
            ((groups, seqs, cols + pair), F32),
            ((seqs * HEADS, KVH * HDIM), F32),
            ((max(seqs, 8), HEADS * HDIM), F32),
        ],
    )
    near_mixed = swap_all([mixed] * groups)
    w_out, fresh = load([w_out, fresh], (2, 1), LOAD_FLOPS, [mixed], out=(1,))
    (outbound,) = call(
        functools.partial(project_out_body, groups=groups, experts=experts, fold=fold),
        [((slots, fold * groups, out_cols // fold), BF16)],
        [*near_mixed, *near_tokens, w_out],
        scratch=[
            ((groups * seqs, width), F32),
            ((2 * seqs, fold * groups, out_cols // fold), F32),
            ((seqs, fold * groups, marked), F32),
        ],
    )
    arrived = lax.all_to_all(outbound, both_axes, 0, 0, tiled=True)
    arrived = arrived.reshape(slots * fold * groups, out_cols // fold)
    other = lax.ppermute(arrived, "tp", [(j, j ^ 1) for j in range(groups)])
    used = chunks + chunks // groups
    height = 4 if 1 <= used % 8 <= 4 else 8
    blocks = -(-used // height)
    (answers,) = call(
        functools.partial(expert_body, groups=groups, experts=experts, fold=fold),
        [((slots, blocks, height, LANES), BF16)],
        [
            arrived,
            other,
            row(mix_gain),
            row(ffn_gain),
            w_gate[0],
            w_lin[0],
            gate_bias,
            lin_bias,
            w_down[0],
        ],
        scratch=[
            ((slots, width), BF16),
            ((slots * blocks * 8, LANES), F32),
        ],
    )
    returned = lax.all_to_all(answers, both_axes, 0, 0, tiled=True)
    (updated,) = call(
        functools.partial(finish_body, groups=groups, experts=experts),
        [((seqs, width), BF16)],
        [returned, own_tokens, combine, pick, block(mix_gain), block(post_gain)],
        hbm_out=(0,),
        scratch=[
            ((max(seqs, 8), width), F32),
            ((chunks, LANES), F32),
            ((chunks, LANES), F32),
        ],
    )
    return (updated, fresh)


def solution(mesh):
    in_specs = (
        P(("ep", "tp"), None),
        P(("ep", "tp"), None, None),
        P(("ep", "tp"), None, None),
        P(("ep", "tp"), None, None),
        P(("ep", "tp")),
        P(("ep", "tp"), None),
        P(("ep", "tp"), None),
        P(),
        P(None, "tp"),
        P(None, "tp"),
        P(),
        P(),
        P(None, "tp"),
        P(),
        P(),
        P("ep", None, "tp"),
        P("ep", None, "tp"),
        P("ep", "tp"),
        P("ep", "tp"),
        P("ep", "tp", None),
        P(),
    )
    out_specs = (P(("ep", "tp"), None), P(("ep", "tp"), None))
    return jax.shard_map(layer, mesh=mesh, in_specs=in_specs, out_specs=out_specs, check_vma=False)
```

profile of v0, /device:TPU:0, one launch (start us, length us, event | category | flops | bytes accessed | tf_op | source)
XLA Modules:
  0.0 44.8 jit_solution(3337051428579268682)
XLA Ops:
  0.7 2.5 %collective-permute-start.2 = (bf16[2,2048]{1,0:T(2,128)(2,1)}, bf16[2,2048]{1,0:T(2,128)(2,1)S(1)}, u32[]{:S(2)}, u32[]{:S(2)}) collective-permute-start(bf16[2,2048]{1,0:T(2,128)(2,1)} %refs_4_.1), channel_id=1, source_target_pairs={{0,3},{1,2},{2,1},{3,0},{4,7},{5,6},{6,5},{7,4},{8,11},{9,10},{10,... | collective-permute-start | bytes 24584 | tf_op jit(solution)/shard_map/ppermute | solution.py:119
  3.2 0.6 %collective-permute-start.1 = (bf16[2,2048]{1,0:T(2,128)(2,1)}, bf16[2,2048]{1,0:T(2,128)(2,1)S(1)}, u32[]{:S(2)}, u32[]{:S(2)}) collective-permute-start(bf16[2,2048]{1,0:T(2,128)(2,1)} %refs_4_.1), channel_id=1, source_target_pairs={{0,2},{1,3},{2,0},{3,1},{4,6},{5,7},{6,4},{7,5},{8,10},{9,11},{10,... | collective-permute-start | bytes 24584 | tf_op jit(solution)/shard_map/ppermute | solution.py:119
  3.8 0.0 collective-permute-start
  3.8 2.0 %shard_map.212 = (bf16[2048,512]{1,0:T(8,128)(2,1)S(1)}, bf16[2048,128]{1,0:T(8,128)(2,1)S(1)}, bf16[2,1024,256]{2,1,0:T(8,128)(2,1)S(1)}) custom-call(bf16[2048,512]{1,0:T(8,128)(2,1)} %refs_0_.3, bf16[2048,128]{1,0:T(8,128)(2,1)} %refs_1_.1, bf16[2,1024,256]{2,1,0:T(8,128)(2,1)} %refs_2_.1), custom_call_target="tpu_custom_call" | custom-call | flops 50000000 | tf_op jit(solution)/shard_map/pallas_call | solution.py:47
  5.9 0.0 copy-start.6
  5.9 0.0 copy-start.7
  5.9 0.0 copy-start.12
  5.9 0.0 copy-start.13
  5.9 0.0 copy-start.14
  6.0 1.1 %collective-permute-done.1.refs_2_.refs_6_ = bf16[2,2048]{1,0:T(2,128)(2,1)S(1)} collective-permute-done((bf16[2,2048]{1,0:T(2,128)(2,1)}, bf16[2,2048]{1,0:T(2,128)(2,1)S(1)}, u32[]{:S(2)}, u32[]{:S(2)}) %collective-permute-start.1) | collective-permute-done | bytes 8224 | tf_op jit(solution)/shard_map/ppermute | solution.py:119
  7.0 0.5 %shard_map.213 = (bf16[2,640]{1,0:T(2,128)(2,1)S(1)}, bf16[2,640]{1,0:T(2,128)(2,1)S(1)}, bf16[2,640]{1,0:T(2,128)(2,1)S(1)}, bf16[2,640]{1,0:T(2,128)(2,1)S(1)}) custom-call(bf16[2,2048]{1,0:T(2,128)(2,1)S(1)} %copy-done.3, bf16[2,2048]{1,0:T(2,128)(2,1)S(1)} %collective-permute-done.refs_1_.refs_5_, ...), custom_call_target="tpu_custom_call" | custom-call | tf_op jit(solution)/shard_map/pallas_call | solution.py:47
  7.6 0.1 collective-permute-start.3
  7.6 0.8 %collective-permute-start.4 = (bf16[2,640]{1,0:T(2,128)(2,1)S(1)}, bf16[2,640]{1,0:T(2,128)(2,1)S(1)}, u32[]{:S(2)}, u32[]{:S(2)}) collective-permute-start(bf16[2,640]{1,0:T(2,128)(2,1)S(1)} %get-tuple-element.24), channel_id=1, source_target_pairs={{0,2},{1,3},{2,0},{3,1},{4,6},{5,7},{6,4},{7,5},{8,10},{9,11},{10,... | collective-permute-start | bytes 7688 | tf_op jit(solution)/shard_map/ppermute | solution.py:119
  8.5 1.0 %collective-permute-start.5 = (bf16[2,640]{1,0:T(2,128)(2,1)S(1)}, bf16[2,640]{1,0:T(2,128)(2,1)S(1)}, u32[]{:S(2)}, u32[]{:S(2)}) collective-permute-start(bf16[2,640]{1,0:T(2,128)(2,1)S(1)} %get-tuple-element.25), channel_id=1, source_target_pairs={{0,3},{1,2},{2,1},{3,0},{4,7},{5,6},{6,5},{7,4},{8,11},{9,10},{10,... | collective-permute-start | bytes 7688 | tf_op jit(solution)/shard_map/ppermute | solution.py:119
  9.5 1.2 %shard_map.214 = (bf16[2,256,1024]{2,1,0:T(8,128)(2,1)S(1)}, bf16[2,1024,256]{2,1,0:T(8,128)(2,1)S(1)}, f32[2,2,1024]{2,1,0:T(2,128)S(1)}, f32[2,128]{1,0:T(2,12...) custom-call(bf16[2,1024,256]{2,1,0:T(8,128)(2,1)S(1)} %get-tuple-element.26.keys, ...), custom_call_target="tpu_custom_call" | custom-call | flops 50000000 | tf_op jit(solution)/shard_map/pallas_call | solution.py:47
  10.8 0.5 %collective-permute-done.4.refs_2_ = bf16[2,640]{1,0:T(2,128)(2,1)S(1)} collective-permute-done((bf16[2,640]{1,0:T(2,128)(2,1)S(1)}, bf16[2,640]{1,0:T(2,128)(2,1)S(1)}, u32[]{:S(2)}, u32[]{:S(2)}) %collective-permute-start.4) | collective-permute-done | bytes 2592 | tf_op jit(solution)/shard_map/ppermute | solution.py:119
  11.3 0.2 collective-permute-done.5.refs_3_
  11.5 0.8 %shard_map.215 = (bf16[2,2176]{1,0:T(2,128)(2,1)S(1)}, bf16[2,512]{1,0:T(2,128)(2,1)S(1)}) custom-call(bf16[2,640]{1,0:T(2,128)(2,1)S(1)} %get-tuple-element.22.after.refs_0_, bf16[2,640]{1,0:T(2,128)(2,1)S(1)} %collective-permute-done.3.refs_1_, bf16[2,640]{1,0:T(2,128)(2,1)S(1)} %collective-permute-done.4.refs_2_, ...), custom_call_target="tpu_custom_call" | custom-call | tf_op jit(solution)/shard_map/pallas_call | solution.py:47
  12.3 1.1 %collective-permute-start.8 = (bf16[2,2176]{1,0:T(2,128)(2,1)S(1)}, bf16[2,2176]{1,0:T(2,128)(2,1)S(1)}, u32[]{:S(2)}, u32[]{:S(2)}) collective-permute-start(bf16[2,2176]{1,0:T(2,128)(2,1)S(1)} %get-tuple-element.31.refs_2_.refs_0_), channel_id=1, source_target_pairs={{0,3},{1,2},{2,1},{3,0},{4,7},{5,6},{6,5},{7,4},{8,11},{9,10},{10,... | collective-permute-start | bytes 26120 | tf_op jit(solution)/shard_map/ppermute | solution.py:119
  13.4 0.7 %collective-permute-start.7 = (bf16[2,2176]{1,0:T(2,128)(2,1)S(1)}, bf16[2,2176]{1,0:T(2,128)(2,1)S(1)}, u32[]{:S(2)}, u32[]{:S(2)}) collective-permute-start(bf16[2,2176]{1,0:T(2,128)(2,1)S(1)} %get-tuple-element.31.refs_2_.refs_0_), channel_id=1, source_target_pairs={{0,2},{1,3},{2,0},{3,1},{4,6},{5,7},{6,4},{7,5},{8,10},{9,11},{10,... | collective-permute-start | bytes 26120 | tf_op jit(solution)/shard_map/ppermute | solution.py:119
  14.1 0.1 collective-permute-start.6
  14.2 0.0 copy-start.11
  14.2 1.7 %shard_map.216 = (bf16[2048,512]{1,0:T(8,128)(2,1)S(1)}, bf16[2,512]{1,0:T(2,128)(2,1)}) custom-call(bf16[2048,512]{1,0:T(8,128)(2,1)} %refs_0_.5, bf16[2,512]{1,0:T(2,128)(2,1)S(1)} %get-tuple-element.32.refs_1_, bf16[2,2176]{1,0:T(2,128)(2,1)S(1)} %get-tuple-element.31.refs_2_.refs_0_), custom_call_target="tpu_custom_call" | custom-call | flops 50000000 | tf_op jit(solution)/shard_map/pallas_call | solution.py:47
  16.0 1.1 %collective-permute-done.7.refs_2_ = bf16[2,2176]{1,0:T(2,128)(2,1)S(1)} collective-permute-done((bf16[2,2176]{1,0:T(2,128)(2,1)S(1)}, bf16[2,2176]{1,0:T(2,128)(2,1)S(1)}, u32[]{:S(2)}, u32[]{:S(2)}) %collective-permute-start.7) | collective-permute-done | bytes 8736 | tf_op jit(solution)/shard_map/ppermute | solution.py:119
  17.0 0.4 shard_map.217
  17.5 13.1 %all_to_all.10 = bf16[32,8,256]{2,1,0:T(8,128)(2,1)S(1)} all-to-all(bf16[32,8,256]{2,1,0:T(8,128)(2,1)S(1)} %shard_map.217), channel_id=1, replica_groups=mesh['ep'=8,'tp'=4] {'ep','tp'}, dimensions={0} | all-to-all | bytes 262144 | tf_op jit(solution)/shard_map/all_to_all | solution.py:476
  30.5 0.2 collective-permute-start.9
  30.7 1.1 %collective-permute-done.9.other = bf16[256,256]{1,0:T(8,128)(2,1)S(1)} collective-permute-done((bf16[256,256]{1,0:T(8,128)(2,1)S(1)}, bf16[256,256]{1,0:T(8,128)(2,1)S(1)}, u32[]{:S(2)}, u32[]{:S(2)}) %collective-permute-start.9) | collective-permute-done | bytes 131104 | tf_op jit(solution)/shard_map/ppermute | solution.py:478
  31.9 0.0 copy-start.9
  31.9 1.5 %shard_map.218 = bf16[32,5,4,128]{3,2,1,0:T(4,128)(2,1)S(1)} custom-call(bf16[256,256]{1,0:T(8,128)(2,1)S(1)} %bitcast.16, bf16[256,256]{1,0:T(8,128)(2,1)S(1)} %collective-permute-done.9.other, f32[1,2048]{1,0:T(1,128)S(1)} %bitcast.19, f32[1,2048]{1,0:T(1,128)S(1)} %bitcast.22, bf16[2048,512]{1,0:T(8,128)(2,1)S(1)} %bitcast.12, ...), custom_call_target="tpu_custom_call" | custom-call | tf_op jit(solution)/shard_map/pallas_call | solution.py:47
  33.5 10.4 %all_to_all.11.returned = bf16[32,5,4,128]{3,2,1,0:T(4,128)(2,1)S(1)} all-to-all(bf16[32,5,4,128]{3,2,1,0:T(4,128)(2,1)S(1)} %shard_map.218), channel_id=1, replica_groups=mesh['ep'=8,'tp'=4] {'ep','tp'}, dimensions={0} | all-to-all | bytes 327680 | tf_op jit(solution)/shard_map/all_to_all | solution.py:501
  43.9 0.9 %shard_map.219 = bf16[2,2048]{1,0:T(2,128)(2,1)} custom-call(bf16[32,5,4,128]{3,2,1,0:T(4,128)(2,1)S(1)} %all_to_all.11.returned, f32[32,128]{1,0:T(8,128)S(1)} %get-tuple-element.34.tokens, f32[2,128]{1,0:T(2,128)S(1)} %get-tuple-element.35.combine, f32[2,128]{1,0:T(2,128)S(1)} %get-tuple-element.36.pick, f32[16,128]{1,0:T(8,128)S(1)} %bitcast.20, ...), custom_call_target="tpu_custom_call" | custom-call | tf_op jit(solution)/shard_map/pallas_call | solution.py:47
  (30 shorter events, 0.1 us)
Async XLA Ops:
  0.6 6.4 %copy-start.3 = (bf16[2,2048]{1,0:T(2,128)(2,1)S(1)}, bf16[2,2048]{1,0:T(2,128)(2,1)}, u32[]{:S(2)}) copy-start(bf16[2,2048]{1,0:T(2,128)(2,1)} %refs_4_.1) | copy-start | bytes 24580
  0.6 6.4 %copy-start.4 = (f32[2048]{0:T(1024)S(1)}, f32[2048]{0:T(1024)}, u32[]{:S(2)}) copy-start(f32[2048]{0:T(1024)} %param.28) | copy-start | bytes 24580
  0.7 5.3 %collective-permute-start.2 = (bf16[2,2048]{1,0:T(2,128)(2,1)}, bf16[2,2048]{1,0:T(2,128)(2,1)S(1)}, u32[]{:S(2)}, u32[]{:S(2)}) collective-permute-start(bf16[2,2048]{1,0:T(2,128)(2,1)} %refs_4_.1), channel_id=1, source_target_pairs={{0,3},{1,2},{2,1},{3,0},{4,7},{5,6},{6,5},{7,4},{8,11},{9,10},{10,... | collective-permute-start | bytes 24584 | tf_op jit(solution)/shard_map/ppermute | solution.py:119
  3.2 3.9 %collective-permute-start.1 = (bf16[2,2048]{1,0:T(2,128)(2,1)}, bf16[2,2048]{1,0:T(2,128)(2,1)S(1)}, u32[]{:S(2)}, u32[]{:S(2)}) collective-permute-start(bf16[2,2048]{1,0:T(2,128)(2,1)} %refs_4_.1), channel_id=1, source_target_pairs={{0,2},{1,3},{2,0},{3,1},{4,6},{5,7},{6,4},{7,5},{8,10},{9,11},{10,... | collective-permute-start | bytes 24584 | tf_op jit(solution)/shard_map/ppermute | solution.py:119
  3.8 3.2 %collective-permute-start = (bf16[2,2048]{1,0:T(2,128)(2,1)}, bf16[2,2048]{1,0:T(2,128)(2,1)S(1)}, u32[]{:S(2)}, u32[]{:S(2)}) collective-permute-start(bf16[2,2048]{1,0:T(2,128)(2,1)} %refs_4_.1), channel_id=1, source_target_pairs={{0,1},{1,0},{2,3},{3,2},{4,5},{5,4},{6,7},{7,6},{8,9},{9,8},{10,11... | collective-permute-start | bytes 24584 | tf_op jit(solution)/shard_map/ppermute | solution.py:119
  5.9 3.6 %copy-start.6 = (f32[2,2,1024]{2,1,0:T(2,128)S(1)}, f32[2,2,1024]{2,1,0:T(2,128)}, u32[]{:S(2)}) copy-start(f32[2,2,1024]{2,1,0:T(2,128)} %gates.1) | copy-start | bytes 49156
  5.9 3.6 %copy-start.7 = (bf16[2048,2]{0,1:T(2,128)(2,1)S(1)}, bf16[2048,2]{0,1:T(2,128)(2,1)}, u32[]{:S(2)}) copy-start(bf16[2048,2]{0,1:T(2,128)(2,1)} %param.31) | copy-start | bytes 24580
  5.9 3.6 %copy-start.12 = (s32[2,4]{1,0:T(2,128)S(1)}, s32[2,4]{1,0:T(2,128)}, u32[]{:S(2)}) copy-start(s32[2,4]{1,0:T(2,128)} %routes.1) | copy-start | bytes 100
  5.9 3.6 %copy-start.13 = (f32[2,4]{1,0:T(2,128)S(1)}, f32[2,4]{1,0:T(2,128)}, u32[]{:S(2)}) copy-start(f32[2,4]{1,0:T(2,128)} %logits.1) | copy-start | bytes 100
  5.9 3.6 %copy-start.14 = (s32[2]{0:T(128)S(1)}, s32[2]{0:T(128)}, u32[]{:S(2)}) copy-start(s32[2]{0:T(128)} %param.25) | copy-start | bytes 28
  5.9 3.6 %copy-start.15 = (f32[2]{0:T(128)S(1)}, f32[2]{0:T(128)}, u32[]{:S(2)}) copy-start(f32[2]{0:T(128)} %param.32) | copy-start | bytes 28
  7.6 3.2 %collective-permute-start.3 = (bf16[2,640]{1,0:T(2,128)(2,1)S(1)}, bf16[2,640]{1,0:T(2,128)(2,1)S(1)}, u32[]{:S(2)}, u32[]{:S(2)}) collective-permute-start(bf16[2,640]{1,0:T(2,128)(2,1)S(1)} %get-tuple-element.23), channel_id=1, source_target_pairs={{0,1},{1,0},{2,3},{3,2},{4,5},{5,4},{6,7},{7,6},{8,9},{9,8},{10,11... | collective-permute-start | bytes 7688 | tf_op jit(solution)/shard_map/ppermute | solution.py:119
  7.6 3.7 %collective-permute-start.4 = (bf16[2,640]{1,0:T(2,128)(2,1)S(1)}, bf16[2,640]{1,0:T(2,128)(2,1)S(1)}, u32[]{:S(2)}, u32[]{:S(2)}) collective-permute-start(bf16[2,640]{1,0:T(2,128)(2,1)S(1)} %get-tuple-element.24), channel_id=1, source_target_pairs={{0,2},{1,3},{2,0},{3,1},{4,6},{5,7},{6,4},{7,5},{8,10},{9,11},{10,... | collective-permute-start | bytes 7688 | tf_op jit(solution)/shard_map/ppermute | solution.py:119
  8.5 3.0 %collective-permute-start.5 = (bf16[2,640]{1,0:T(2,128)(2,1)S(1)}, bf16[2,640]{1,0:T(2,128)(2,1)S(1)}, u32[]{:S(2)}, u32[]{:S(2)}) collective-permute-start(bf16[2,640]{1,0:T(2,128)(2,1)S(1)} %get-tuple-element.25), channel_id=1, source_target_pairs={{0,3},{1,2},{2,1},{3,0},{4,7},{5,6},{6,5},{7,4},{8,11},{9,10},{10,... | collective-permute-start | bytes 7688 | tf_op jit(solution)/shard_map/ppermute | solution.py:119
  11.5 20.4 %copy-start.2 = (bf16[1,512,2048]{2,1,0:T(8,128)(2,1)S(1)}, bf16[1,512,2048]{2,1,0:T(8,128)(2,1)}, u32[]{:S(2)}) copy-start(bf16[1,512,2048]{2,1,0:T(8,128)(2,1)} %param.40) | copy-start | bytes 6291460
  12.3 3.7 %collective-permute-start.8 = (bf16[2,2176]{1,0:T(2,128)(2,1)S(1)}, bf16[2,2176]{1,0:T(2,128)(2,1)S(1)}, u32[]{:S(2)}, u32[]{:S(2)}) collective-permute-start(bf16[2,2176]{1,0:T(2,128)(2,1)S(1)} %get-tuple-element.31.refs_2_.refs_0_), channel_id=1, source_target_pairs={{0,3},{1,2},{2,1},{3,0},{4,7},{5,6},{6,5},{7,4},{8,11},{9,10},{10,... | collective-permute-start | bytes 26120 | tf_op jit(solution)/shard_map/ppermute | solution.py:119
  13.4 3.7 %collective-permute-start.7 = (bf16[2,2176]{1,0:T(2,128)(2,1)S(1)}, bf16[2,2176]{1,0:T(2,128)(2,1)S(1)}, u32[]{:S(2)}, u32[]{:S(2)}) collective-permute-start(bf16[2,2176]{1,0:T(2,128)(2,1)S(1)} %get-tuple-element.31.refs_2_.refs_0_), channel_id=1, source_target_pairs={{0,2},{1,3},{2,0},{3,1},{4,6},{5,7},{6,4},{7,5},{8,10},{9,11},{10,... | collective-permute-start | bytes 26120 | tf_op jit(solution)/shard_map/ppermute | solution.py:119
  14.1 2.9 %collective-permute-start.6 = (bf16[2,2176]{1,0:T(2,128)(2,1)S(1)}, bf16[2,2176]{1,0:T(2,128)(2,1)S(1)}, u32[]{:S(2)}, u32[]{:S(2)}) collective-permute-start(bf16[2,2176]{1,0:T(2,128)(2,1)S(1)} %get-tuple-element.31.refs_2_.refs_0_), channel_id=1, source_target_pairs={{0,1},{1,0},{2,3},{3,2},{4,5},{5,4},{6,7},{7,6},{8,9},{9,8},{10,11... | collective-permute-start | bytes 26120 | tf_op jit(solution)/shard_map/ppermute | solution.py:119
  14.2 17.7 %copy-start = (bf16[1,2048,512]{2,1,0:T(8,128)(2,1)S(1)}, bf16[1,2048,512]{2,1,0:T(8,128)(2,1)}, u32[]{:S(2)}) copy-start(bf16[1,2048,512]{2,1,0:T(8,128)(2,1)} %param.36) | copy-start | bytes 6291460
  14.2 17.7 %copy-start.1 = (bf16[1,2048,512]{2,1,0:T(8,128)(2,1)S(1)}, bf16[1,2048,512]{2,1,0:T(8,128)(2,1)}, u32[]{:S(2)}) copy-start(bf16[1,2048,512]{2,1,0:T(8,128)(2,1)} %param.37) | copy-start | bytes 6291460
  14.2 17.7 %copy-start.5 = (f32[2048]{0:T(1024)S(1)}, f32[2048]{0:T(1024)}, u32[]{:S(2)}) copy-start(f32[2048]{0:T(1024)} %param.34) | copy-start | bytes 24580
  14.2 17.7 %copy-start.8 = (f32[2048]{0:T(1024)S(1)}, f32[2048]{0:T(1024)}, u32[]{:S(2)}) copy-start(f32[2048]{0:T(1024)} %param.35) | copy-start | bytes 24580
  14.2 17.7 %copy-start.10 = (f32[1,512]{1,0:T(1,128)S(1)}, f32[1,512]{1,0:T(1,128)}, u32[]{:S(2)}) copy-start(f32[1,512]{1,0:T(1,128)} %gate_bias.1) | copy-start | bytes 6148
  14.2 17.7 %copy-start.11 = (f32[1,512]{1,0:T(1,128)S(1)}, f32[1,512]{1,0:T(1,128)}, u32[]{:S(2)}) copy-start(f32[1,512]{1,0:T(1,128)} %lin_bias.1) | copy-start | bytes 6148
  30.5 1.3 %collective-permute-start.9 = (bf16[256,256]{1,0:T(8,128)(2,1)S(1)}, bf16[256,256]{1,0:T(8,128)(2,1)S(1)}, u32[]{:S(2)}, u32[]{:S(2)}) collective-permute-start(bf16[256,256]{1,0:T(8,128)(2,1)S(1)} %bitcast.15), channel_id=1, source_target_pairs={{0,1},{1,0},{2,3},{3,2},{4,5},{5,4},{6,7},{7,6},{8,9},{9,8},{10,11... | collective-permute-start | bytes 393224 | tf_op jit(solution)/shard_map/ppermute | solution.py:478
  31.9 11.9 %copy-start.9 = (f32[2048]{0:T(1024)S(1)}, f32[2048]{0:T(1024)}, u32[]{:S(2)}) copy-start(f32[2048]{0:T(1024)} %param.41) | copy-start | bytes 24580
where the time goes:
time: 45 us; the launch traced here: 44.8 us
  blocking collectives  23.4 us (52%)
  Pallas kernels  9.2 us (20%)
  starting transfers between devices  7.23 us (16%)
  waiting for transfers between devices  3.94 us (9%)
  between operations  0.87 us (2%)
    all_to_all x1, blocking collectives, layer(): arrived = lax.all_to_all(outbound, both_axes, 0, 0, tiled=True)  13.1 us
    all_to_all x1, blocking collectives, layer(): returned = lax.all_to_all(answers, both_axes, 0, 0, tiled=True)  10.4 us
    pallas_call x8, Pallas kernels, call(): pl.pallas_call(body, out_shape=[jax.ShapeDtypeStruct(shape, dtype) if i i...  9.2 us
    ppermute x9, starting transfers between devices, swap_all(): out.append(lax.ppermute(pieces[k], 'tp', perm))  7.01 us
    ppermute x9, waiting for transfers between devices, swap_all(): out.append(lax.ppermute(pieces[k], 'tp', perm))  2.81 us
    ppermute x1, waiting for transfers between devices, layer(): other = lax.ppermute(arrived, 'tp', [(j, j ^ 1) for j in range(groups)])  1.13 us
  transfers between devices with their start and end apart: 10, of which 5 were waited for; matrix products, arithmetic and copies ran while one was open for 0% of the time, Pallas kernels for 11%

commit v1 on v0

--- a/solution.py
+++ b/solution.py
@@ -202,23 +202,25 @@
                 c, s : s + 1, at : at + HDIM
             ]
     head = lax.broadcasted_iota(jnp.int32, (HEADS, 1), 0)
+    queries = [q_rows[s * HEADS : (s + 1) * HEADS, :] for s in range(seqs)]
+    raws = [jnp.dot(queries[s].astype(BF16), keys[s], preferred_element_type=F32) for s in range(seqs)]
+    weights, own_weights = [], []
     for s in range(seqs):
-        query = q_rows[s * HEADS : (s + 1) * HEADS, :]
         new_key = fresh[s : s + 1, : KVH * HDIM]
-        new_value = fresh[s : s + 1, KVH * HDIM :]
-        raw = jnp.dot(query.astype(BF16), keys[s], preferred_element_type=F32)
         row_bias = bias[s, KVH - 1 : KVH, :]
         for g in range(KVH - 1):
             row_bias = jnp.where((head >= g * share) & (head < (g + 1) * share), bias[s, g : g + 1, :], row_bias)
-        scores = raw * scale + row_bias
-        own = jnp.sum(query * new_key, axis=-1, keepdims=True) * scale
+        scores = raws[s] * scale + row_bias
+        own = jnp.sum(queries[s] * new_key, axis=-1, keepdims=True) * scale
         top = jnp.maximum(jnp.max(scores, axis=-1, keepdims=True), own)
         expo = jnp.exp(scores - top)
         own_expo = jnp.exp(own - top)
         total = 1.0 / (jnp.sum(expo, axis=-1, keepdims=True) + own_expo)
-        weight = (expo * total).astype(BF16)
-        own_weight = (own_expo * total).astype(BF16).astype(F32)
-        mixed = jnp.dot(weight, values[s], preferred_element_type=F32) + own_weight * new_value
+        weights.append((expo * total).astype(BF16))
+        own_weights.append((own_expo * total).astype(BF16).astype(F32))
+    products = [jnp.dot(weights[s], values[s], preferred_element_type=F32) for s in range(seqs)]
+    for s in range(seqs):
+        mixed = products[s] + own_weights[s] * fresh[s : s + 1, KVH * HDIM :]
         for h in range(HEADS):
             g = h // share
             mixed_rows[s : s + 1, h * HDIM : (h + 1) * HDIM] = mixed[
@@ -279,7 +281,6 @@
     side = chunks // groups
     per = lanes // LANES
     blocks, height = out.shape[1:3]
-    pitch = blocks * 8
     even = (here & 1) == 0
 
     def tile(slot, c):
@@ -290,8 +291,13 @@
         mine, theirs = arrived[spot].astype(F32), other[spot].astype(F32)
         return jnp.where(even, mine, theirs), jnp.where(even, theirs, mine)
 
-    def spot(chunk):
-        return chunk // height * 8 + chunk % height
+    def put(chunk, first, values):
+        block, row = chunk // height, chunk % height
+        answer[block, pl.ds(first * 8 + row, values.shape[0], stride=8), :] = values
+
+    def close(block):
+        for slot in range(groups * experts):
+            out[slot, block] = answer[block, slot * 8 : slot * 8 + height, :].astype(BF16)
 
     if blocks * height > chunks + side:
         answer[...] = jnp.zeros(answer.shape, F32)
@@ -317,22 +323,28 @@
         for c in range(per):
             tiles = [tile(i * groups + here, c)[0] for i in near]
             for a in range(fold):
-                answer[pl.ds(at * pitch + spot(chunks + a * per + c), count, stride=pitch), :] = (
-                    jnp.concatenate([t[a * groups : (a + 1) * groups] for t in tiles], axis=0)
-                )
+                mine = jnp.concatenate([t[a * groups : (a + 1) * groups] for t in tiles], axis=0)
+                put(chunks + a * per + c, at, mine)
     rows = expert_in[...]
-    gate = jnp.dot(rows, w_gate[...], preferred_element_type=F32) + gate_bias[...]
-    linear = jnp.dot(rows, w_lin[...], preferred_element_type=F32) + lin_bias[...]
-    act = clamped_unit(gate, linear).astype(BF16)
-    part = jnp.dot(act, w_down[...], preferred_element_type=F32)
-    for c in range(chunks):
-        answer[pl.ds(spot(c), groups * experts, stride=pitch), :] = part[
-            :, c * LANES : (c + 1) * LANES
-        ]
-    for slot in range(groups * experts):
-        for b in range(blocks):
-            at = slot * pitch + b * 8
-            out[slot, b] = answer[at : at + height, :].astype(BF16)
+    hidden = w_gate.shape[1]
+    cut = hidden // 2 if hidden % (4 * LANES) == 0 else hidden
+    acts = []
+    for at in range(0, hidden, cut):
+        span = slice(at, at + cut)
+        gate = jnp.dot(rows, w_gate[:, span], preferred_element_type=F32) + gate_bias[:, span]
+        linear = jnp.dot(rows, w_lin[:, span], preferred_element_type=F32) + lin_bias[:, span]
+        acts.append(clamped_unit(gate, linear).astype(BF16))
+    act = jnp.concatenate(acts, axis=1)
+    for block in range(chunks // height, blocks):
+        close(block)
+    wide = height * LANES
+    for block in range(chunks // height):
+        part = jnp.dot(
+            act, w_down[:, block * wide : (block + 1) * wide], preferred_element_type=F32
+        )
+        for c in range(height):
+            put(block * height + c, 0, part[:, c * LANES : (c + 1) * LANES])
+        close(block)
 
 
 def finish_body(
@@ -495,7 +507,7 @@
         ],
         scratch=[
             ((slots, width), BF16),
-            ((slots * blocks * 8, LANES), F32),
+            ((blocks, slots * 8, LANES), F32),
         ],
     )
     returned = lax.all_to_all(answers, both_axes, 0, 0, tiled=True)

time: 45 us -> 44.8 us (level)
  no operation moved by 1% of the time
where the time goes in v1:
time: 44.8 us; the launch traced here: 44.6 us
  blocking collectives  23.4 us (52%)
  Pallas kernels  9.03 us (20%)
  starting transfers between devices  7.23 us (16%)
  waiting for transfers between devices  3.94 us (9%)
  between operations  0.87 us (2%)
    all_to_all x1, blocking collectives, layer(): arrived = lax.all_to_all(outbound, both_axes, 0, 0, tiled=True)  13.1 us
    all_to_all x1, blocking collectives, layer(): returned = lax.all_to_all(answers, both_axes, 0, 0, tiled=True)  10.4 us
    pallas_call x8, Pallas kernels, call(): pl.pallas_call(body, out_shape=[jax.ShapeDtypeStruct(shape, dtype) if i i...  9.03 us
    ppermute x9, starting transfers between devices, swap_all(): out.append(lax.ppermute(pieces[k], 'tp', perm))  7.01 us
    ppermute x9, waiting for transfers between devices, swap_all(): out.append(lax.ppermute(pieces[k], 'tp', perm))  2.81 us
    ppermute x1, waiting for transfers between devices, layer(): other = lax.ppermute(arrived, 'tp', [(j, j ^ 1) for j in range(groups)])  1.13 us
  transfers between devices with their start and end apart: 10, of which 5 were waited for; matrix products, arithmetic and copies ran while one was open for 0% of the time, Pallas kernels for 11%

profile of v1, /device:TPU:0, one launch (start us, length us, event | category | flops | bytes accessed | tf_op | source)
XLA Modules:
  0.0 44.6 jit_solution(946143905538894969)
XLA Ops:
  0.7 2.5 %collective-permute-start.2 = (bf16[2,2048]{1,0:T(2,128)(2,1)}, bf16[2,2048]{1,0:T(2,128)(2,1)S(1)}, u32[]{:S(2)}, u32[]{:S(2)}) collective-permute-start(bf16[2,2048]{1,0:T(2,128)(2,1)} %refs_4_.1), channel_id=1, source_target_pairs={{0,3},{1,2},{2,1},{3,0},{4,7},{5,6},{6,5},{7,4},{8,11},{9,10},{10,... | collective-permute-start | bytes 24584 | tf_op jit(solution)/shard_map/ppermute | solution.py:119
  3.2 0.6 %collective-permute-start.1 = (bf16[2,2048]{1,0:T(2,128)(2,1)}, bf16[2,2048]{1,0:T(2,128)(2,1)S(1)}, u32[]{:S(2)}, u32[]{:S(2)}) collective-permute-start(bf16[2,2048]{1,0:T(2,128)(2,1)} %refs_4_.1), channel_id=1, source_target_pairs={{0,2},{1,3},{2,0},{3,1},{4,6},{5,7},{6,4},{7,5},{8,10},{9,11},{10,... | collective-permute-start | bytes 24584 | tf_op jit(solution)/shard_map/ppermute | solution.py:119
  3.8 0.0 collective-permute-start
  3.8 2.0 %shard_map.212 = (bf16[2048,512]{1,0:T(8,128)(2,1)S(1)}, bf16[2048,128]{1,0:T(8,128)(2,1)S(1)}, bf16[2,1024,256]{2,1,0:T(8,128)(2,1)S(1)}) custom-call(bf16[2048,512]{1,0:T(8,128)(2,1)} %refs_0_.3, bf16[2048,128]{1,0:T(8,128)(2,1)} %refs_1_.1, bf16[2,1024,256]{2,1,0:T(8,128)(2,1)} %refs_2_.1), custom_call_target="tpu_custom_call" | custom-call | flops 50000000 | tf_op jit(solution)/shard_map/pallas_call | solution.py:47
  5.9 0.0 copy-start.6
  5.9 0.0 copy-start.7
  5.9 0.0 copy-start.12
  5.9 0.0 copy-start.13
  5.9 0.0 copy-start.14
  5.9 0.0 copy-start.15
  6.0 1.1 %collective-permute-done.1.refs_2_.refs_6_ = bf16[2,2048]{1,0:T(2,128)(2,1)S(1)} collective-permute-done((bf16[2,2048]{1,0:T(2,128)(2,1)}, bf16[2,2048]{1,0:T(2,128)(2,1)S(1)}, u32[]{:S(2)}, u32[]{:S(2)}) %collective-permute-start.1) | collective-permute-done | bytes 8224 | tf_op jit(solution)/shard_map/ppermute | solution.py:119
  7.0 0.5 %shard_map.213 = (bf16[2,640]{1,0:T(2,128)(2,1)S(1)}, bf16[2,640]{1,0:T(2,128)(2,1)S(1)}, bf16[2,640]{1,0:T(2,128)(2,1)S(1)}, bf16[2,640]{1,0:T(2,128)(2,1)S(1)}) custom-call(bf16[2,2048]{1,0:T(2,128)(2,1)S(1)} %copy-done.3, bf16[2,2048]{1,0:T(2,128)(2,1)S(1)} %collective-permute-done.refs_1_.refs_5_, ...), custom_call_target="tpu_custom_call" | custom-call | tf_op jit(solution)/shard_map/pallas_call | solution.py:47
  7.6 0.1 collective-permute-start.3
  7.6 0.8 %collective-permute-start.4 = (bf16[2,640]{1,0:T(2,128)(2,1)S(1)}, bf16[2,640]{1,0:T(2,128)(2,1)S(1)}, u32[]{:S(2)}, u32[]{:S(2)}) collective-permute-start(bf16[2,640]{1,0:T(2,128)(2,1)S(1)} %get-tuple-element.24), channel_id=1, source_target_pairs={{0,2},{1,3},{2,0},{3,1},{4,6},{5,7},{6,4},{7,5},{8,10},{9,11},{10,... | collective-permute-start | bytes 7688 | tf_op jit(solution)/shard_map/ppermute | solution.py:119
  8.5 1.0 %collective-permute-start.5 = (bf16[2,640]{1,0:T(2,128)(2,1)S(1)}, bf16[2,640]{1,0:T(2,128)(2,1)S(1)}, u32[]{:S(2)}, u32[]{:S(2)}) collective-permute-start(bf16[2,640]{1,0:T(2,128)(2,1)S(1)} %get-tuple-element.25), channel_id=1, source_target_pairs={{0,3},{1,2},{2,1},{3,0},{4,7},{5,6},{6,5},{7,4},{8,11},{9,10},{10,... | collective-permute-start | bytes 7688 | tf_op jit(solution)/shard_map/ppermute | solution.py:119
  9.5 1.2 %shard_map.214 = (bf16[2,256,1024]{2,1,0:T(8,128)(2,1)S(1)}, bf16[2,1024,256]{2,1,0:T(8,128)(2,1)S(1)}, f32[2,2,1024]{2,1,0:T(2,128)S(1)}, f32[2,128]{1,0:T(2,12...) custom-call(bf16[2,1024,256]{2,1,0:T(8,128)(2,1)S(1)} %get-tuple-element.26.keys, ...), custom_call_target="tpu_custom_call" | custom-call | flops 50000000 | tf_op jit(solution)/shard_map/pallas_call | solution.py:47
  10.8 0.5 %collective-permute-done.4.refs_2_ = bf16[2,640]{1,0:T(2,128)(2,1)S(1)} collective-permute-done((bf16[2,640]{1,0:T(2,128)(2,1)S(1)}, bf16[2,640]{1,0:T(2,128)(2,1)S(1)}, u32[]{:S(2)}, u32[]{:S(2)}) %collective-permute-start.4) | collective-permute-done | bytes 2592 | tf_op jit(solution)/shard_map/ppermute | solution.py:119
  11.3 0.2 collective-permute-done.5.refs_3_
  11.5 0.7 %shard_map.215 = (bf16[2,2176]{1,0:T(2,128)(2,1)S(1)}, bf16[2,512]{1,0:T(2,128)(2,1)S(1)}) custom-call(bf16[2,640]{1,0:T(2,128)(2,1)S(1)} %get-tuple-element.22.after.refs_0_, bf16[2,640]{1,0:T(2,128)(2,1)S(1)} %collective-permute-done.3.refs_1_, bf16[2,640]{1,0:T(2,128)(2,1)S(1)} %collective-permute-done.4.refs_2_, ...), custom_call_target="tpu_custom_call" | custom-call | tf_op jit(solution)/shard_map/pallas_call | solution.py:47
  12.1 1.1 %collective-permute-start.8 = (bf16[2,2176]{1,0:T(2,128)(2,1)S(1)}, bf16[2,2176]{1,0:T(2,128)(2,1)S(1)}, u32[]{:S(2)}, u32[]{:S(2)}) collective-permute-start(bf16[2,2176]{1,0:T(2,128)(2,1)S(1)} %get-tuple-element.31.refs_2_.refs_0_), channel_id=1, source_target_pairs={{0,3},{1,2},{2,1},{3,0},{4,7},{5,6},{6,5},{7,4},{8,11},{9,10},{10,... | collective-permute-start | bytes 26120 | tf_op jit(solution)/shard_map/ppermute | solution.py:119
  13.2 0.7 %collective-permute-start.7 = (bf16[2,2176]{1,0:T(2,128)(2,1)S(1)}, bf16[2,2176]{1,0:T(2,128)(2,1)S(1)}, u32[]{:S(2)}, u32[]{:S(2)}) collective-permute-start(bf16[2,2176]{1,0:T(2,128)(2,1)S(1)} %get-tuple-element.31.refs_2_.refs_0_), channel_id=1, source_target_pairs={{0,2},{1,3},{2,0},{3,1},{4,6},{5,7},{6,4},{7,5},{8,10},{9,11},{10,... | collective-permute-start | bytes 26120 | tf_op jit(solution)/shard_map/ppermute | solution.py:119
  14.0 0.1 collective-permute-start.6
  14.1 0.0 copy-start.11
  14.1 1.7 %shard_map.216 = (bf16[2048,512]{1,0:T(8,128)(2,1)S(1)}, bf16[2,512]{1,0:T(2,128)(2,1)}) custom-call(bf16[2048,512]{1,0:T(8,128)(2,1)} %refs_0_.5, bf16[2,512]{1,0:T(2,128)(2,1)S(1)} %get-tuple-element.32.refs_1_, bf16[2,2176]{1,0:T(2,128)(2,1)S(1)} %get-tuple-element.31.refs_2_.refs_0_), custom_call_target="tpu_custom_call" | custom-call | flops 50000000 | tf_op jit(solution)/shard_map/pallas_call | solution.py:47
  15.9 1.1 %collective-permute-done.7.refs_2_ = bf16[2,2176]{1,0:T(2,128)(2,1)S(1)} collective-permute-done((bf16[2,2176]{1,0:T(2,128)(2,1)S(1)}, bf16[2,2176]{1,0:T(2,128)(2,1)S(1)}, u32[]{:S(2)}, u32[]{:S(2)}) %collective-permute-start.7) | collective-permute-done | bytes 8736 | tf_op jit(solution)/shard_map/ppermute | solution.py:119
  16.9 0.4 shard_map.217
  17.3 13.1 %all_to_all.10 = bf16[32,8,256]{2,1,0:T(8,128)(2,1)S(1)} all-to-all(bf16[32,8,256]{2,1,0:T(8,128)(2,1)S(1)} %shard_map.217), channel_id=1, replica_groups=mesh['ep'=8,'tp'=4] {'ep','tp'}, dimensions={0} | all-to-all | bytes 262144 | tf_op jit(solution)/shard_map/all_to_all | solution.py:488
  30.4 0.2 collective-permute-start.9
  30.6 1.1 %collective-permute-done.9.other = bf16[256,256]{1,0:T(8,128)(2,1)S(1)} collective-permute-done((bf16[256,256]{1,0:T(8,128)(2,1)S(1)}, bf16[256,256]{1,0:T(8,128)(2,1)S(1)}, u32[]{:S(2)}, u32[]{:S(2)}) %collective-permute-start.9) | collective-permute-done | bytes 131104 | tf_op jit(solution)/shard_map/ppermute | solution.py:490
  31.8 1.5 %shard_map.218 = bf16[32,5,4,128]{3,2,1,0:T(4,128)(2,1)S(1)} custom-call(bf16[256,256]{1,0:T(8,128)(2,1)S(1)} %bitcast.16, bf16[256,256]{1,0:T(8,128)(2,1)S(1)} %collective-permute-done.9.other, f32[1,2048]{1,0:T(1,128)S(1)} %bitcast.19, f32[1,2048]{1,0:T(1,128)S(1)} %bitcast.22, bf16[2048,512]{1,0:T(8,128)(2,1)S(1)} %bitcast.12, ...), custom_call_target="tpu_custom_call" | custom-call | tf_op jit(solution)/shard_map/pallas_call | solution.py:47
  33.3 10.4 %all_to_all.11.returned = bf16[32,5,4,128]{3,2,1,0:T(4,128)(2,1)S(1)} all-to-all(bf16[32,5,4,128]{3,2,1,0:T(4,128)(2,1)S(1)} %shard_map.218), channel_id=1, replica_groups=mesh['ep'=8,'tp'=4] {'ep','tp'}, dimensions={0} | all-to-all | bytes 327680 | tf_op jit(solution)/shard_map/all_to_all | solution.py:513
  43.7 0.9 %shard_map.219 = bf16[2,2048]{1,0:T(2,128)(2,1)} custom-call(bf16[32,5,4,128]{3,2,1,0:T(4,128)(2,1)S(1)} %all_to_all.11.returned, f32[32,128]{1,0:T(8,128)S(1)} %get-tuple-element.34.tokens, f32[2,128]{1,0:T(2,128)S(1)} %get-tuple-element.35.combine, f32[2,128]{1,0:T(2,128)S(1)} %get-tuple-element.36.pick, f32[16,128]{1,0:T(8,128)S(1)} %bitcast.20, ...), custom_call_target="tpu_custom_call" | custom-call | tf_op jit(solution)/shard_map/pallas_call | solution.py:47
  (30 shorter events, 0.1 us)
Async XLA Ops:
  0.6 6.4 %copy-start.3 = (bf16[2,2048]{1,0:T(2,128)(2,1)S(1)}, bf16[2,2048]{1,0:T(2,128)(2,1)}, u32[]{:S(2)}) copy-start(bf16[2,2048]{1,0:T(2,128)(2,1)} %refs_4_.1) | copy-start | bytes 24580
  0.6 6.4 %copy-start.4 = (f32[2048]{0:T(1024)S(1)}, f32[2048]{0:T(1024)}, u32[]{:S(2)}) copy-start(f32[2048]{0:T(1024)} %param.28) | copy-start | bytes 24580
  0.7 5.3 %collective-permute-start.2 = (bf16[2,2048]{1,0:T(2,128)(2,1)}, bf16[2,2048]{1,0:T(2,128)(2,1)S(1)}, u32[]{:S(2)}, u32[]{:S(2)}) collective-permute-start(bf16[2,2048]{1,0:T(2,128)(2,1)} %refs_4_.1), channel_id=1, source_target_pairs={{0,3},{1,2},{2,1},{3,0},{4,7},{5,6},{6,5},{7,4},{8,11},{9,10},{10,... | collective-permute-start | bytes 24584 | tf_op jit(solution)/shard_map/ppermute | solution.py:119
  3.2 3.9 %collective-permute-start.1 = (bf16[2,2048]{1,0:T(2,128)(2,1)}, bf16[2,2048]{1,0:T(2,128)(2,1)S(1)}, u32[]{:S(2)}, u32[]{:S(2)}) collective-permute-start(bf16[2,2048]{1,0:T(2,128)(2,1)} %refs_4_.1), channel_id=1, source_target_pairs={{0,2},{1,3},{2,0},{3,1},{4,6},{5,7},{6,4},{7,5},{8,10},{9,11},{10,... | collective-permute-start | bytes 24584 | tf_op jit(solution)/shard_map/ppermute | solution.py:119
  3.8 3.2 %collective-permute-start = (bf16[2,2048]{1,0:T(2,128)(2,1)}, bf16[2,2048]{1,0:T(2,128)(2,1)S(1)}, u32[]{:S(2)}, u32[]{:S(2)}) collective-permute-start(bf16[2,2048]{1,0:T(2,128)(2,1)} %refs_4_.1), channel_id=1, source_target_pairs={{0,1},{1,0},{2,3},{3,2},{4,5},{5,4},{6,7},{7,6},{8,9},{9,8},{10,11... | collective-permute-start | bytes 24584 | tf_op jit(solution)/shard_map/ppermute | solution.py:119
  5.9 3.6 %copy-start.6 = (f32[2,2,1024]{2,1,0:T(2,128)S(1)}, f32[2,2,1024]{2,1,0:T(2,128)}, u32[]{:S(2)}) copy-start(f32[2,2,1024]{2,1,0:T(2,128)} %gates.1) | copy-start | bytes 49156
  5.9 3.6 %copy-start.7 = (bf16[2048,2]{0,1:T(2,128)(2,1)S(1)}, bf16[2048,2]{0,1:T(2,128)(2,1)}, u32[]{:S(2)}) copy-start(bf16[2048,2]{0,1:T(2,128)(2,1)} %param.31) | copy-start | bytes 24580
  5.9 3.6 %copy-start.12 = (s32[2,4]{1,0:T(2,128)S(1)}, s32[2,4]{1,0:T(2,128)}, u32[]{:S(2)}) copy-start(s32[2,4]{1,0:T(2,128)} %routes.1) | copy-start | bytes 100
  5.9 3.6 %copy-start.13 = (f32[2,4]{1,0:T(2,128)S(1)}, f32[2,4]{1,0:T(2,128)}, u32[]{:S(2)}) copy-start(f32[2,4]{1,0:T(2,128)} %logits.1) | copy-start | bytes 100
  5.9 3.6 %copy-start.14 = (s32[2]{0:T(128)S(1)}, s32[2]{0:T(128)}, u32[]{:S(2)}) copy-start(s32[2]{0:T(128)} %param.25) | copy-start | bytes 28
  5.9 3.6 %copy-start.15 = (f32[2]{0:T(128)S(1)}, f32[2]{0:T(128)}, u32[]{:S(2)}) copy-start(f32[2]{0:T(128)} %param.32) | copy-start | bytes 28
  7.6 3.2 %collective-permute-start.3 = (bf16[2,640]{1,0:T(2,128)(2,1)S(1)}, bf16[2,640]{1,0:T(2,128)(2,1)S(1)}, u32[]{:S(2)}, u32[]{:S(2)}) collective-permute-start(bf16[2,640]{1,0:T(2,128)(2,1)S(1)} %get-tuple-element.23), channel_id=1, source_target_pairs={{0,1},{1,0},{2,3},{3,2},{4,5},{5,4},{6,7},{7,6},{8,9},{9,8},{10,11... | collective-permute-start | bytes 7688 | tf_op jit(solution)/shard_map/ppermute | solution.py:119
  7.6 3.7 %collective-permute-start.4 = (bf16[2,640]{1,0:T(2,128)(2,1)S(1)}, bf16[2,640]{1,0:T(2,128)(2,1)S(1)}, u32[]{:S(2)}, u32[]{:S(2)}) collective-permute-start(bf16[2,640]{1,0:T(2,128)(2,1)S(1)} %get-tuple-element.24), channel_id=1, source_target_pairs={{0,2},{1,3},{2,0},{3,1},{4,6},{5,7},{6,4},{7,5},{8,10},{9,11},{10,... | collective-permute-start | bytes 7688 | tf_op jit(solution)/shard_map/ppermute | solution.py:119
  8.5 3.0 %collective-permute-start.5 = (bf16[2,640]{1,0:T(2,128)(2,1)S(1)}, bf16[2,640]{1,0:T(2,128)(2,1)S(1)}, u32[]{:S(2)}, u32[]{:S(2)}) collective-permute-start(bf16[2,640]{1,0:T(2,128)(2,1)S(1)} %get-tuple-element.25), channel_id=1, source_target_pairs={{0,3},{1,2},{2,1},{3,0},{4,7},{5,6},{6,5},{7,4},{8,11},{9,10},{10,... | collective-permute-start | bytes 7688 | tf_op jit(solution)/shard_map/ppermute | solution.py:119
  11.5 20.3 %copy-start.2 = (bf16[1,512,2048]{2,1,0:T(8,128)(2,1)S(1)}, bf16[1,512,2048]{2,1,0:T(8,128)(2,1)}, u32[]{:S(2)}) copy-start(bf16[1,512,2048]{2,1,0:T(8,128)(2,1)} %param.40) | copy-start | bytes 6291460
  12.1 3.7 %collective-permute-start.8 = (bf16[2,2176]{1,0:T(2,128)(2,1)S(1)}, bf16[2,2176]{1,0:T(2,128)(2,1)S(1)}, u32[]{:S(2)}, u32[]{:S(2)}) collective-permute-start(bf16[2,2176]{1,0:T(2,128)(2,1)S(1)} %get-tuple-element.31.refs_2_.refs_0_), channel_id=1, source_target_pairs={{0,3},{1,2},{2,1},{3,0},{4,7},{5,6},{6,5},{7,4},{8,11},{9,10},{10,... | collective-permute-start | bytes 26120 | tf_op jit(solution)/shard_map/ppermute | solution.py:119
  13.2 3.7 %collective-permute-start.7 = (bf16[2,2176]{1,0:T(2,128)(2,1)S(1)}, bf16[2,2176]{1,0:T(2,128)(2,1)S(1)}, u32[]{:S(2)}, u32[]{:S(2)}) collective-permute-start(bf16[2,2176]{1,0:T(2,128)(2,1)S(1)} %get-tuple-element.31.refs_2_.refs_0_), channel_id=1, source_target_pairs={{0,2},{1,3},{2,0},{3,1},{4,6},{5,7},{6,4},{7,5},{8,10},{9,11},{10,... | collective-permute-start | bytes 26120 | tf_op jit(solution)/shard_map/ppermute | solution.py:119
  14.0 2.9 %collective-permute-start.6 = (bf16[2,2176]{1,0:T(2,128)(2,1)S(1)}, bf16[2,2176]{1,0:T(2,128)(2,1)S(1)}, u32[]{:S(2)}, u32[]{:S(2)}) collective-permute-start(bf16[2,2176]{1,0:T(2,128)(2,1)S(1)} %get-tuple-element.31.refs_2_.refs_0_), channel_id=1, source_target_pairs={{0,1},{1,0},{2,3},{3,2},{4,5},{5,4},{6,7},{7,6},{8,9},{9,8},{10,11... | collective-permute-start | bytes 26120 | tf_op jit(solution)/shard_map/ppermute | solution.py:119
  14.1 17.7 %copy-start = (bf16[1,2048,512]{2,1,0:T(8,128)(2,1)S(1)}, bf16[1,2048,512]{2,1,0:T(8,128)(2,1)}, u32[]{:S(2)}) copy-start(bf16[1,2048,512]{2,1,0:T(8,128)(2,1)} %param.36) | copy-start | bytes 6291460
  14.1 17.7 %copy-start.1 = (bf16[1,2048,512]{2,1,0:T(8,128)(2,1)S(1)}, bf16[1,2048,512]{2,1,0:T(8,128)(2,1)}, u32[]{:S(2)}) copy-start(bf16[1,2048,512]{2,1,0:T(8,128)(2,1)} %param.37) | copy-start | bytes 6291460
  14.1 17.7 %copy-start.5 = (f32[2048]{0:T(1024)S(1)}, f32[2048]{0:T(1024)}, u32[]{:S(2)}) copy-start(f32[2048]{0:T(1024)} %param.34) | copy-start | bytes 24580
  14.1 17.7 %copy-start.8 = (f32[2048]{0:T(1024)S(1)}, f32[2048]{0:T(1024)}, u32[]{:S(2)}) copy-start(f32[2048]{0:T(1024)} %param.35) | copy-start | bytes 24580
  14.1 17.7 %copy-start.10 = (f32[1,512]{1,0:T(1,128)S(1)}, f32[1,512]{1,0:T(1,128)}, u32[]{:S(2)}) copy-start(f32[1,512]{1,0:T(1,128)} %gate_bias.1) | copy-start | bytes 6148
  14.1 17.7 %copy-start.11 = (f32[1,512]{1,0:T(1,128)S(1)}, f32[1,512]{1,0:T(1,128)}, u32[]{:S(2)}) copy-start(f32[1,512]{1,0:T(1,128)} %lin_bias.1) | copy-start | bytes 6148
  30.4 1.3 %collective-permute-start.9 = (bf16[256,256]{1,0:T(8,128)(2,1)S(1)}, bf16[256,256]{1,0:T(8,128)(2,1)S(1)}, u32[]{:S(2)}, u32[]{:S(2)}) collective-permute-start(bf16[256,256]{1,0:T(8,128)(2,1)S(1)} %bitcast.15), channel_id=1, source_target_pairs={{0,1},{1,0},{2,3},{3,2},{4,5},{5,4},{6,7},{7,6},{8,9},{9,8},{10,11... | collective-permute-start | bytes 393224 | tf_op jit(solution)/shard_map/ppermute | solution.py:490
  31.8 11.9 %copy-start.9 = (f32[2048]{0:T(1024)S(1)}, f32[2048]{0:T(1024)}, u32[]{:S(2)}) copy-start(f32[2048]{0:T(1024)} %param.41) | copy-start | bytes 24580
